TPU v7x, 32 devices: a whole 2x2x4 slice. The times are simulated.
32 devices in a mesh: sp: 16 (over z, y, x), tp: 2 (over core).
Axes of the slice: x: 2, y: 2, z: 4, core: 2. Of those that a mesh axis runs over, the one named last changes fastest.
Arguments:
- queries: bfloat16 [4096, 1024], P('sp', 'tp'), may hold values from -6 to 6
- keys: bfloat16 [4096, 512], P('sp', 'tp'), may hold values from -6 to 6
- values: bfloat16 [4096, 512], P('sp', 'tp'), may hold values from -6 to 6
- q_gain: float32 [64], replicated, may hold values from 1.6 to 4.5
- key_norm_gain: float32 [64], replicated, may hold values from 1.6 to 4.5
- out_weight: bfloat16 [1024, 2048], P('tp'), may hold values from -0.1875 to 0.1875
- residual: bfloat16 [4096, 2048], P('sp'), may hold values from -6 to 6
- ln1_gain: float32 [2048], replicated, may hold values from 0.1 to 1.9
- ln1_bias: float32 [2048], replicated, may hold values from -3 to 3
- up_weight: bfloat16 [2048, 8192], P('sp', 'tp'), may hold values from -0.125 to 0.125
- down_weight: bfloat16 [8192, 2048], P('tp', 'sp'), may hold values from -0.0625 to 0.0625
- ln2_gain: float32 [2048], replicated, may hold values from 0.1 to 1.9
- ln2_bias: float32 [2048], replicated, may hold values from -3 to 3
Outputs:
- encoded: bfloat16 [4096, 2048], P('sp', 'tp')
All inputs are finite; a program needn't handle non-finite values.
Results may differ from a plain program's by a relative error of at most 0.014.
Values may be sent and summed in bfloat16 or wider, within the bound.
A program may use at most 128 MiB of HBM per device.

v0:
```python
import math

import jax
import jax.numpy as jnp
from jax import lax
from jax.sharding import PartitionSpec as P

D = 2048
HEAD_SIZE = 64
GRID_W = 64


ALPHA = 8.0**0.25
ROTARY_BASE = 10000.0
RMS_EPSILON = 1e-06
NORM_EPSILON = 1e-05


def rotate_grid(heads_in, grid_places):
    half_dim = heads_in.shape[-1] // 2
    quarter = half_dim // 2
    inverse = ROTARY_BASE ** (-jnp.arange(quarter, dtype=jnp.float32) / quarter)

    def spin(segment, coords):
        angles = coords.astype(jnp.float32)[:, None] * inverse[None, :]
        cos_val = jnp.cos(angles)[:, None, :]
        sin_val = jnp.sin(angles)[:, None, :]
        lead_half = segment[..., :quarter]
        tail_half = segment[..., quarter:]
        return jnp.concatenate(
            [lead_half * cos_val - tail_half * sin_val, tail_half * cos_val + lead_half * sin_val],
            -1,
        )

    return jnp.concatenate(
        [
            spin(heads_in[..., :half_dim], grid_places // GRID_W),
            spin(heads_in[..., half_dim:], grid_places % GRID_W),
        ],
        -1,
    )


def prepare_inputs(heads_in, gain_vec, grid_places, factor):
    values32 = heads_in.astype(jnp.float32)
    normed = (
        values32
        * lax.rsqrt(jnp.mean(values32 * values32, -1, keepdims=True) + RMS_EPSILON)
        * gain_vec
    )
    return (rotate_grid(normed, grid_places) * factor).astype(jnp.bfloat16)


def layer_norm(pre_norm, gain_vec, bias_vec):
    row_mean = jnp.mean(pre_norm, -1, keepdims=True)
    centred = pre_norm - row_mean
    spread = jnp.mean(centred * centred, -1, keepdims=True)
    return centred * lax.rsqrt(spread + NORM_EPSILON) * gain_vec + bias_vec


def finish_norm(pre_norm, stats, gain_vec, bias_vec):
    row_mean = stats[0][:, None] / D
    spread = stats[1][:, None] / D - row_mean * row_mean
    return (pre_norm - row_mean) * lax.rsqrt(spread + NORM_EPSILON) * gain_vec + bias_vec


def take_cols(array_in, col_start, col_width):
    return lax.dynamic_slice_in_dim(array_in, col_start, col_width, array_in.ndim - 1)


def local(
    queries,
    keys,
    values,
    q_gain,
    key_norm_gain,
    out_weight,
    residual,
    ln1_gain,
    ln1_bias,
    up_weight,
    down_weight,
    ln2_gain,
    ln2_bias,
):
    tok_rows = queries.shape[0]
    grid_places = lax.axis_index("sp") * tok_rows + jnp.arange(tok_rows, dtype=jnp.int32)
    kv_heads = keys.shape[1] // HEAD_SIZE
    q_count = queries.shape[1] // HEAD_SIZE
    group_count_size = q_count // kv_heads
    query_head_rows = prepare_inputs(
        queries.reshape(tok_rows, q_count, HEAD_SIZE), q_gain, grid_places, HEAD_SIZE ** (-0.5)
    )
    q_grouped = query_head_rows.reshape(tok_rows, kv_heads, group_count_size, HEAD_SIZE)
    k_sent = prepare_inputs(
        keys.reshape(tok_rows, kv_heads, HEAD_SIZE), key_norm_gain, grid_places, 1.0
    ).reshape(tok_rows, kv_heads * HEAD_SIZE)
    initial = (
        jnp.full((kv_heads, group_count_size, tok_rows), -jnp.inf, jnp.float32),
        jnp.zeros((kv_heads, group_count_size, tok_rows), jnp.float32),
        jnp.zeros((tok_rows, kv_heads, group_count_size, HEAD_SIZE), jnp.float32),
    )
    key_piece = lax.all_gather(k_sent, "sp", axis=0, tiled=True)
    value_piece = lax.all_gather(values, "sp", axis=0, tiled=True)
    key_count = key_piece.shape[0]
    block_len = math.gcd(key_count, 2048)
    key_blocks = key_piece.reshape(key_count // block_len, block_len, kv_heads, HEAD_SIZE)
    value_blocks = value_piece.reshape(key_count // block_len, block_len, kv_heads, HEAD_SIZE)

    def advance(state_in, blocks):
        maxima, totals, accumulated = state_in
        scores = jnp.einsum(
            "qhgd,khd->hgqk", q_grouped, blocks[0], preferred_element_type=jnp.float32
        )
        new_max = jnp.maximum(maxima, jnp.max(scores, -1))
        factor = jnp.exp(maxima - new_max)
        weights = jnp.exp(scores - new_max[..., None])
        totals = totals * factor + jnp.sum(weights, -1)
        update = jnp.einsum(
            "hgqk,khd->qhgd",
            weights.astype(jnp.bfloat16),
            blocks[1],
            preferred_element_type=jnp.float32,
        )
        accumulated = accumulated * jnp.transpose(factor, (2, 0, 1))[..., None] + update
        return ((new_max, totals, accumulated), None)

    state_out, unused = lax.scan(advance, initial, (key_blocks, value_blocks))
    maxima, totals, accumulated = state_out
    attended = (
        (accumulated / jnp.transpose(totals, (2, 0, 1))[..., None])
        .reshape(tok_rows, q_count * HEAD_SIZE)
        .astype(jnp.bfloat16)
    )
    partial_value = jnp.dot(attended, out_weight, preferred_element_type=jnp.float32)
    col_width = D // lax.axis_size("tp")
    col_start = lax.axis_index("tp") * col_width
    mixed_sum = lax.psum(partial_value.astype(jnp.bfloat16), "tp").astype(jnp.float32)
    full_rows = layer_norm(
        ALPHA * residual.astype(jnp.float32) + mixed_sum, ln1_gain, ln1_bias
    ).astype(jnp.bfloat16)
    normed_own = take_cols(full_rows, col_start, col_width)
    up_acts = jnp.dot(
        full_rows,
        lax.all_gather(up_weight, "sp", axis=0, tiled=True),
        preferred_element_type=jnp.float32,
    )
    hidden = jnp.square(jnp.maximum(up_acts, 0.0)).astype(jnp.bfloat16)
    partial_ffn = jnp.dot(
        hidden,
        lax.all_gather(down_weight, "sp", axis=1, tiled=True),
        preferred_element_type=jnp.float32,
    )
    ffn_cols = lax.psum_scatter(
        partial_ffn.astype(jnp.bfloat16), "tp", scatter_dimension=1, tiled=True
    ).astype(jnp.float32)
    second = ALPHA * normed_own.astype(jnp.float32) + ffn_cols
    stats_two = lax.psum((jnp.sum(second, -1), jnp.sum(second * second, -1)), "tp")
    return finish_norm(
        second,
        stats_two,
        take_cols(ln2_gain, col_start, col_width),
        take_cols(ln2_bias, col_start, col_width),
    ).astype(jnp.bfloat16)


def solution(mesh):
    return jax.shard_map(
        local,
        mesh=mesh,
        in_specs=(
            P("sp", "tp"),
            P("sp", "tp"),
            P("sp", "tp"),
            P(),
            P(),
            P("tp", None),
            P("sp", None),
            P(),
            P(),
            P("sp", "tp"),
            P("tp", "sp"),
            P(),
            P(),
        ),
        out_specs=P("sp", "tp"),
        check_vma=False,
    )
```

profile of v0, /device:TPU:0, one launch (start us, length us, event | category | flops | bytes accessed | tf_op | source)
XLA Modules:
  0.0 704.4 jit_solution(7267192037591548552)
XLA Ops:
  6.5 0.0 copy-start
  6.5 0.0 copy-start.6
  6.5 0.0 all-gather.5.cloned.1.call-start
  6.6 1.1 copy.21
  7.8 0.7 fusion.30
  8.5 0.2 multiply_cosine_fusion.1
  8.8 0.7 pad_maximum_fusion
  9.4 0.0 all-gather.5.cloned.1.call-update
  9.5 0.0 all-gather.7.cloned.1.call-start
  9.5 0.7 all-gather.7.cloned.1.call-update
  10.2 0.0 all-reduce.3.cloned.1.call-start
  10.3 1.1 copy.22
  11.4 0.1 fusion.26
  11.5 0.0 copy-done.6
  11.5 0.1 fusion.27
  11.6 0.1 multiply_subtract_fusion.1
  11.7 65.8 %all-gather.5.cloned.1.call-done = bf16[4096,256]{0,1:T(8,128)(2,1)} async-done(((bf16[256,256]{0,1:T(8,128)(2,1)}), bf16[4096,256]{0,1:T(8,128)(2,1)}) %all-gather.5.cloned.1.call-update) | async-done | bytes 2097168 | tf_op jit(solution)/shard_map/all_gather | solution.py:103
  77.5 4.5 reshape.201
  82.0 3.8 copy.24
  85.8 53.3 %all-gather.7.cloned.1.call-done = bf16[4096,256]{1,0:T(8,128)(2,1)} async-done(((bf16[256,256]{1,0:T(8,128)(2,1)}), bf16[4096,256]{1,0:T(8,128)(2,1)}) %all-gather.7.cloned.1.call-update) | async-done | bytes 2097168 | tf_op jit(solution)/shard_map/all_gather | solution.py:104
  139.1 7.1 %reshape.207 = bf16[2,2048,4,64]{3,2,1,0:T(4,128)(2,1)} reshape(bf16[4096,256]{1,0:T(8,128)(2,1)} %all-gather.7.cloned.1.call-done) | data formatting | bytes 4194304 | tf_op jit(solution)/shard_map/reshape | solution.py:108
  146.2 6.9 copy.25
  153.1 49.9 %while.15 = (s32[]{:T(128)}, f32[4,2,256]{2,1,0:T(2,128)S(1)}, f32[4,2,256]{2,1,0:T(2,128)S(1)}, f32[256,4,2,64]{0,3,2,1:T(8,128)S(1)}, bf16[2,2048,4,64]{1,3,2,...) while((s32[]{:T(128)}, f32[4,2,256]{2,1,0:T(2,128)S(1)}, ...), condition=%wide.region_5.6_spmd.clone, body=%wide.region_2.5_spmd.clone.sunk | while | flops 1095118848 | bytes 53871716 | solution.py:128
  153.1 9.3 %bitcast_reduce_fusion.2 = (f32[4,2,256]{2,1,0:T(2,128)S(1)}, f32[4,2048,256,2]{2,1,3,0:T(8,128)}) fusion(bf16[256,4,2,64]{0,3,2,1:T(8,128)(2,1)S(1)} %get-tuple-element.194, bf16[2,2048,4,64]{1,3,2,0:T(8,128)(2,1)} %get-tuple-element.193, s32[]{:T(128)} %get-tuple-element.180), kind=kOutput, calls=%fused_computation.1.clone.1 | convolution fusion | flops 541063168 | bytes 18096640 | tf_op jit(solution)/shard_map/while/body/eval_jaxpr/qhgd,khd->hgqk/dot_general | solution.py:112
  162.5 7.6 %fusion.55 = f32[256,4,2,64]{0,3,2,1:T(8,128)S(1)} fusion(f32[4,2048,256,2]{2,1,3,0:T(8,128)} %get-tuple-element.169, f32[4,2,256]{2,1,0:T(2,128)S(1)} %get-tuple-element.190, bf16[2,2048,4,64]{1,3,2,0:T(8,128)(2,1)} %get-tuple-element.195, s32[]{:T(128)} %get-tuple-element.180, f32[256,4,2,64]{0,3,2,1:T(8,128)S(1)} %get-tuple-element.183, ...), kind=kOutput, calls=%fused_computation.8.clone.1 | convolution fusion | flops 545652736 | bytes 18891264 | tf_op jit(solution)/shard_map/while/body/eval_jaxpr/hgqk,khd->qhgd/dot_general | solution.py:119
  170.1 8.0 %fusion.53 = f32[4,2,256]{2,1,0:T(2,128)S(1)} fusion(f32[4,2048,256,2]{2,1,3,0:T(8,128)} %get-tuple-element.169, f32[4,2,256]{2,1,0:T(2,128)S(1)} %get-tuple-element.190), kind=kLoop, calls=%fused_computation.4.clone.1 | loop fusion | flops 8386560 | bytes 16793600 | tf_op jit(solution)/shard_map/while/body/eval_jaxpr/reduce_sum | solution.py:118
  178.1 9.3 %bitcast_reduce_fusion.2 = (f32[4,2,256]{2,1,0:T(2,128)S(1)}, f32[4,2048,256,2]{2,1,3,0:T(8,128)}) fusion(bf16[256,4,2,64]{0,3,2,1:T(8,128)(2,1)S(1)} %get-tuple-element.194, bf16[2,2048,4,64]{1,3,2,0:T(8,128)(2,1)} %get-tuple-element.193, s32[]{:T(128)} %get-tuple-element.180), kind=kOutput, calls=%fused_computation.1.clone.1 | convolution fusion | flops 541063168 | bytes 18096640 | tf_op jit(solution)/shard_map/while/body/eval_jaxpr/qhgd,khd->hgqk/dot_general | solution.py:112
  187.5 7.6 %fusion.55 = f32[256,4,2,64]{0,3,2,1:T(8,128)S(1)} fusion(f32[4,2048,256,2]{2,1,3,0:T(8,128)} %get-tuple-element.169, f32[4,2,256]{2,1,0:T(2,128)S(1)} %get-tuple-element.190, bf16[2,2048,4,64]{1,3,2,0:T(8,128)(2,1)} %get-tuple-element.195, s32[]{:T(128)} %get-tuple-element.180, f32[256,4,2,64]{0,3,2,1:T(8,128)S(1)} %get-tuple-element.183, ...), kind=kOutput, calls=%fused_computation.8.clone.1 | convolution fusion | flops 545652736 | bytes 18891264 | tf_op jit(solution)/shard_map/while/body/eval_jaxpr/hgqk,khd->qhgd/dot_general | solution.py:119
  195.0 8.0 %fusion.53 = f32[4,2,256]{2,1,0:T(2,128)S(1)} fusion(f32[4,2048,256,2]{2,1,3,0:T(8,128)} %get-tuple-element.169, f32[4,2,256]{2,1,0:T(2,128)S(1)} %get-tuple-element.190), kind=kLoop, calls=%fused_computation.4.clone.1 | loop fusion | flops 8386560 | bytes 16793600 | tf_op jit(solution)/shard_map/while/body/eval_jaxpr/reduce_sum | solution.py:118
  203.1 0.0 copy-done
  203.1 1.7 convolution_convert_fusion.1
  204.9 0.0 all-reduce.3.cloned.1.call-update
  204.9 0.0 all-gather.11.cloned.1.call-start
  204.9 0.5 all-gather.11.cloned.1.call-update
  205.5 0.0 all-gather.9.cloned.1.call-start
  205.5 0.5 all-gather.9.cloned.1.call-update
  206.1 0.0 copy-start.2
  206.1 0.0 copy-start.3
  206.1 0.2 reduce-scatter.2.cloned.1.call-start
  206.3 17.0 %all-reduce.3.cloned.1.call-done = bf16[256,2048]{1,0:T(8,128)(2,1)} async-done(((bf16[256,2048]{1,0:T(8,128)(2,1)}), bf16[256,2048]{1,0:T(8,128)(2,1)}) %all-reduce.3.cloned.1.call-update) | async-done | bytes 1048592 | tf_op jit(solution)/shard_map/psum | solution.py:138
  223.3 0.0 copy-start.1
  223.3 2.0 fusion.24
  225.3 0.0 copy-done.1
  225.4 1.8 multiply_reduce_fusion
  227.1 0.0 copy-done.2
  227.2 0.0 copy-done.3
  227.2 2.8 add_convert_fusion
  230.0 0.0 copy-start.4
  230.0 0.0 copy-start.5
  230.0 246.2 %all-gather.11.cloned.1.call-done = bf16[4096,2048]{1,0:T(8,128)(2,1)} async-done(((bf16[4096,128]{1,0:T(8,128)(2,1)}), bf16[4096,2048]{1,0:T(8,128)(2,1)}) %all-gather.11.cloned.1.call-update) | async-done | bytes 16777232 | tf_op jit(solution)/shard_map/all_gather | solution.py:151
  476.2 191.8 %all-gather.9.cloned.1.call-done = bf16[2048,4096]{1,0:T(8,128)(2,1)} async-done(((bf16[128,4096]{1,0:T(8,128)(2,1)}), bf16[2048,4096]{1,0:T(8,128)(2,1)}) %all-gather.9.cloned.1.call-update) | async-done | bytes 16777232 | tf_op jit(solution)/shard_map/all_gather | solution.py:145
  668.0 16.5 %convolution_convert_fusion = bf16[256,2048]{1,0:T(8,128)(2,1)} fusion(bf16[4096,2048]{1,0:T(8,128)(2,1)} %all-gather.11.cloned.1.call-done, bf16[256,2048]{1,0:T(8,128)(2,1)} %add_convert_fusion, bf16[2048,4096]{1,0:T(8,128)(2,1)} %all-gather.9.cloned.1.call-done), kind=kOutput, calls=%fused_computation.26 | convolution fusion | flops 8593604608 | bytes 35651584 | tf_op jit(solution)/shard_map/dot_general | solution.py:149
  684.5 0.0 reduce-scatter.2.cloned.1.call-update
  684.5 0.0 copy-done.4
  684.5 0.0 copy-done.5
  684.6 6.7 reduce-scatter.2.cloned.1.call-done
  691.2 1.5 fusion.25
  692.8 2.5 all-reduce
  695.3 2.3 add_convert_fusion.1
  (22 shorter events, 0.3 us)
Async XLA Ops:
  6.5 196.6 %copy-start = (bf16[512,2048]{1,0:T(8,128)(2,1)S(1)}, bf16[512,2048]{1,0:T(8,128)(2,1)}, u32[]{:S(2)}) copy-start(bf16[512,2048]{1,0:T(8,128)(2,1)} %param.20) | copy-start | bytes 6291460
  6.5 4.9 copy-start.6
  6.5 71.0 %all-gather.5.cloned.1.call-start = ((), (), s32[]{:S(2)}) async-start(), calls=%async_computation.1 | async-start | bytes 2228224 | tf_op jit(solution)/shard_map/all_gather | solution.py:103
  9.5 129.6 %all-gather.7.cloned.1.call-start = ((), (), s32[]{:S(2)}) async-start(), calls=%async_computation.2 | async-start | bytes 2228224 | tf_op jit(solution)/shard_map/all_gather | solution.py:104
  10.2 213.1 %all-reduce.3.cloned.1.call-start = ((), (), s32[]{:S(2)}) async-start(), calls=%async_computation.3 | async-start | bytes 2097152 | tf_op jit(solution)/shard_map/psum | solution.py:138
  204.9 271.3 %all-gather.11.cloned.1.call-start = ((), (), s32[]{:S(2)}) async-start(), calls=%async_computation.5 | async-start | bytes 17825792 | tf_op jit(solution)/shard_map/all_gather | solution.py:151
  205.5 462.5 %all-gather.9.cloned.1.call-start = ((), (), s32[]{:S(2)}) async-start(), calls=%async_computation.4 | async-start | bytes 17825792 | tf_op jit(solution)/shard_map/all_gather | solution.py:145
  206.1 21.1 %copy-start.2 = (f32[2048]{0:T(1024)S(1)}, f32[2048]{0:T(1024)}, u32[]{:S(2)}) copy-start(f32[2048]{0:T(1024)} %param.23) | copy-start | bytes 24580
  206.1 21.1 %copy-start.3 = (f32[2048]{0:T(1024)S(1)}, f32[2048]{0:T(1024)}, u32[]{:S(2)}) copy-start(f32[2048]{0:T(1024)} %param.22) | copy-start | bytes 24580
  206.1 485.2 %reduce-scatter.2.cloned.1.call-start = ((), (), s32[]{:S(2)}) async-start(), calls=%async_computation.6 | async-start | bytes 1572864 | tf_op jit(solution)/shard_map/reduce_scatter | solution.py:154
  223.3 2.1 copy-start.1
  230.0 454.5 %copy-start.4 = (f32[2048]{0:T(1024)S(1)}, f32[2048]{0:T(1024)}, u32[]{:S(2)}) copy-start(f32[2048]{0:T(1024)} %param.26) | copy-start | bytes 24580
  230.0 454.5 %copy-start.5 = (f32[2048]{0:T(1024)S(1)}, f32[2048]{0:T(1024)}, u32[]{:S(2)}) copy-start(f32[2048]{0:T(1024)} %param.27) | copy-start | bytes 24580
Sparse Core Ops, SparseCore 0:
  10.1 67.4 all-gather.4
  80.3 58.7 all-gather.6
  205.0 18.2 all-reduce.2
  225.8 250.2 all-gather.10
  478.8 189.1 all-gather.8
  684.6 6.5 reduce-scatter.1
where the time goes:
time: 705 us; the launch traced here: 704 us
  waiting for transfers between devices  583 us (83%)
  matrix products  52 us (7%)
  other arithmetic  28.7 us (4%)
  local copies, waits for them, and re-layouts  24.6 us (3%)
  between operations  13.7 us (2%)
    all_gather x1, waiting for transfers between devices, local(): lax.all_gather(down_weight, 'sp', axis=1, tiled=True)  246 us
    all_gather x1, waiting for transfers between devices, local(): lax.all_gather(up_weight, 'sp', axis=0, tiled=True)  192 us
    all_gather x1, waiting for transfers between devices, local(): key_piece = lax.all_gather(k_sent, 'sp', axis=0, tiled=True)  65.8 us
    all_gather x1, waiting for transfers between devices, local(): value_piece = lax.all_gather(values, 'sp', axis=0, tiled=True)  53.3 us
    dot_general x2, matrix products, advance(): jnp.einsum('qhgd,khd->hgqk', q_grouped, blocks[0], preferred_element_type...  18.7 us
    psum x1, waiting for transfers between devices, local(): lax.psum(partial_value.astype(jnp.bfloat16), 'tp').astype(jnp.float32)  17 us
    dot_general x1, matrix products, local(): jnp.dot(hidden, lax.all_gather(down_weight, 'sp', axis=1, tiled=True), pr...  16.5 us
    reduce_sum x2, other arithmetic, advance(): totals = totals * factor + jnp.sum(weights, -1)  16 us
  transfers between devices with their start and end apart: 6, of which 6 were waited for; matrix products, arithmetic and copies ran while one was open for 2% of the time, Pallas kernels for 0%

commit v1 on v0

v1 whole, which is shorter than its diff:
```python
import functools
import math

import jax
import jax.numpy as jnp
from jax import lax
from jax.experimental import pallas as pl
from jax.experimental.pallas import tpu as pltpu
from jax.sharding import Mesh, PartitionSpec as P

D = 2048
HEAD_SIZE = 64
GRID_W = 64


ALPHA = 8.0**0.25
ROTARY_BASE = 10000.0
RMS_EPSILON = 1e-06
NORM_EPSILON = 1e-05


def rotate_grid(heads_in, grid_places):
    half_dim = heads_in.shape[-1] // 2
    quarter = half_dim // 2
    inverse = ROTARY_BASE ** (-jnp.arange(quarter, dtype=jnp.float32) / quarter)

    def spin(segment, coords):
        angles = coords.astype(jnp.float32)[:, None] * inverse[None, :]
        cos_val = jnp.cos(angles)[:, None, :]
        sin_val = jnp.sin(angles)[:, None, :]
        lead_half = segment[..., :quarter]
        tail_half = segment[..., quarter:]
        return jnp.concatenate(
            [lead_half * cos_val - tail_half * sin_val, tail_half * cos_val + lead_half * sin_val],
            -1,
        )

    return jnp.concatenate(
        [
            spin(heads_in[..., :half_dim], grid_places // GRID_W),
            spin(heads_in[..., half_dim:], grid_places % GRID_W),
        ],
        -1,
    )


def prepare_inputs(heads_in, gain_vec, grid_places, factor):
    values32 = heads_in.astype(jnp.float32)
    normed = (
        values32
        * lax.rsqrt(jnp.mean(values32 * values32, -1, keepdims=True) + RMS_EPSILON)
        * gain_vec
    )
    return (rotate_grid(normed, grid_places) * factor).astype(jnp.bfloat16)


def layer_norm(pre_norm, gain_vec, bias_vec):
    row_mean = jnp.mean(pre_norm, -1, keepdims=True)
    centred = pre_norm - row_mean
    spread = jnp.mean(centred * centred, -1, keepdims=True)
    return centred * lax.rsqrt(spread + NORM_EPSILON) * gain_vec + bias_vec


def attend_kernel(chunk, q_ref, kv_ref, out_ref, vals_ref):
    width = 2 * HEAD_SIZE
    key_count = kv_ref.shape[0]
    rows = q_ref.shape[0]

    @pl.when(pl.program_id(1) == 0)
    def _():
        lane_kv = lax.broadcasted_iota(jnp.int32, (chunk, width), 1)

        @pl.loop(0, key_count // chunk)
        def _(c):
            at = pl.ds(pl.multiple_of(c * chunk, chunk), chunk)
            vals_ref[at, :] = jnp.where(
                lane_kv < HEAD_SIZE, 1.0, kv_ref[at, :].astype(jnp.float32)
            ).astype(jnp.bfloat16)

    lane = lax.broadcasted_iota(jnp.int32, (rows, width), 1)
    both = q_ref[...].astype(jnp.float32)
    results = []
    for head in range(2):
        own = both if head == 0 else pltpu.roll(both, HEAD_SIZE, 1)
        q = jnp.where(lane < HEAD_SIZE, own, 0.0).astype(jnp.bfloat16)
        top = None
        for c in range(key_count // chunk):
            at = pl.ds(c * chunk, chunk)
            scores = lax.dot_general(
                q, kv_ref[at, :], (((1,), (1,)), ((), ())), preferred_element_type=jnp.float32
            )
            peak = jnp.max(scores, -1, keepdims=True)
            new_top = peak if top is None else jnp.maximum(top, peak)
            weights = jnp.exp(scores - new_top).astype(jnp.bfloat16)
            part = jnp.dot(weights, vals_ref[at, :], preferred_element_type=jnp.float32)
            total = part if top is None else total * jnp.exp(top - new_top) + part
            top = new_top
        results.append(total)
    first, second = (t / pltpu.roll(t, HEAD_SIZE, 1) for t in results)
    out_ref[...] = jnp.where(
        lane < HEAD_SIZE, pltpu.roll(first, HEAD_SIZE, 1), second
    ).astype(jnp.bfloat16)


def attend(q, kv, block=256, chunk=2048):
    heads, rows, width = q.shape
    key_count = kv.shape[1]
    block, chunk = math.gcd(rows, block), math.gcd(key_count, chunk)
    return pl.pallas_call(
        functools.partial(attend_kernel, chunk),
        grid=(heads, rows // block),
        in_specs=[
            pl.BlockSpec((None, block, width), lambda h, i: (h, i, 0)),
            pl.BlockSpec((None, key_count, width), lambda h, i: (h, 0, 0)),
        ],
        out_specs=pl.BlockSpec((None, block, width), lambda h, i: (h, i, 0)),
        out_shape=jax.ShapeDtypeStruct(q.shape, jnp.bfloat16),
        scratch_shapes=[pltpu.VMEM((key_count, width), jnp.bfloat16)],
        compiler_params=pltpu.CompilerParams(dimension_semantics=("arbitrary", "arbitrary")),
        cost_estimate=pl.CostEstimate(
            flops=heads * rows * key_count * 16 * HEAD_SIZE,
            bytes_accessed=2 * (2 * q.size + kv.size),
            transcendentals=heads * rows * key_count * 2,
        ),
    )(q, kv)


def local(
    queries,
    keys,
    values,
    q_gain,
    key_norm_gain,
    out_weight,
    residual,
    ln1_gain,
    ln1_bias,
    up_weight,
    down_weight,
    ln2_gain,
    ln2_bias,
):
    tok_rows = queries.shape[0]
    n_a, n_tp = lax.axis_size("a"), lax.axis_size("tp")
    grid_places = lax.axis_index(("w", "a")) * tok_rows + jnp.arange(tok_rows, dtype=jnp.int32)
    kv_heads = keys.shape[1] // HEAD_SIZE
    q_count = queries.shape[1] // HEAD_SIZE
    own_heads = kv_heads // n_a
    query_rows = prepare_inputs(
        queries.reshape(tok_rows, q_count, HEAD_SIZE), q_gain, grid_places, HEAD_SIZE ** (-0.5)
    ).reshape(tok_rows, kv_heads, 2 * HEAD_SIZE)
    key_rows = prepare_inputs(
        keys.reshape(tok_rows, kv_heads, HEAD_SIZE), key_norm_gain, grid_places, 1.0
    )
    value_rows = values.reshape(tok_rows, kv_heads, HEAD_SIZE)
    packed = jnp.concatenate([query_rows, key_rows, value_rows], -1)
    packed = jnp.transpose(packed, (1, 0, 2)).reshape(n_a, own_heads, tok_rows, 4 * HEAD_SIZE)
    packed = lax.all_to_all(packed, "a", 0, 0, tiled=True)
    packed = jnp.transpose(packed, (1, 0, 2, 3)).reshape(
        own_heads, n_a * tok_rows, 4 * HEAD_SIZE
    )
    q = packed[..., : 2 * HEAD_SIZE]
    kv = lax.all_gather(packed[..., 2 * HEAD_SIZE :], "w", axis=1, tiled=True)

    out_full = lax.all_gather(out_weight, "tp", axis=0, tiled=True)
    up_own = lax.all_to_all(up_weight, "a", 1, 0, tiled=True)
    up_full = lax.all_gather(up_own, "w", axis=0, tiled=True)
    down_own = lax.all_to_all(down_weight, "a", 0, 1, tiled=True)
    down_full = lax.all_gather(down_own, "w", axis=0)

    attended = attend(q, kv)
    rows = tok_rows // n_tp
    sent = attended.reshape(own_heads, n_a * n_tp, rows, 2 * HEAD_SIZE)
    sent = jnp.transpose(sent, (1, 0, 2, 3))
    got = lax.all_to_all(sent, ("a", "tp"), 0, 0, tiled=True)
    got = got.reshape(n_a, n_tp, own_heads, rows, 2 * HEAD_SIZE)
    group_cols = jnp.transpose(got, (1, 3, 0, 2, 4)).reshape(n_tp, rows, -1)
    out_groups = out_full.reshape(2, -1, D)
    both = jnp.transpose(group_cols, (1, 0, 2)).reshape(rows, 2, -1)
    mixed = sum(
        jnp.dot(both[:, g], out_groups[g], preferred_element_type=jnp.float32)
        .astype(jnp.bfloat16)
        .astype(jnp.float32)
        for g in range(2)
    )
    own_residual = lax.dynamic_slice_in_dim(residual, lax.axis_index("tp") * rows, rows, 0)
    normed = layer_norm(
        ALPHA * own_residual.astype(jnp.float32) + mixed, ln1_gain, ln1_bias
    ).astype(jnp.bfloat16)
    full_rows = lax.all_gather(normed, ("a", "tp"), axis=0, tiled=True)
    up_acts = jnp.dot(full_rows, up_full, preferred_element_type=jnp.float32)
    hidden = jnp.square(jnp.maximum(up_acts, 0.0)).astype(jnp.bfloat16)
    partial_ffn = jnp.concatenate(
        [
            jnp.dot(hidden, down_full[i], preferred_element_type=jnp.float32).astype(jnp.bfloat16)
            for i in range(down_full.shape[0])
        ],
        -1,
    )
    ffn_out = lax.psum_scatter(
        partial_ffn, ("a", "tp"), scatter_dimension=0, tiled=True
    ).astype(jnp.float32)
    encoded = layer_norm(
        ALPHA * normed.astype(jnp.float32) + ffn_out, ln2_gain, ln2_bias
    ).astype(jnp.bfloat16)
    return lax.all_to_all(encoded, "tp", 1, 0, tiled=True)


def solution(mesh):
    n_sp, n_tp = mesh.shape["sp"], mesh.shape["tp"]

    def layer(queries, keys, *others):
        n_a = math.gcd(n_sp, keys.shape[1] // (HEAD_SIZE * n_tp))
        groups = Mesh(mesh.devices.reshape(n_sp // n_a, n_a, n_tp), ("w", "a", "tp"))
        sp = ("w", "a")
        cut = P(sp, "tp")
        return jax.shard_map(
            local,
            mesh=groups,
            in_specs=(cut, cut, cut, P(), P(), P("tp", None), P(sp, None), P(), P())
            + (cut, P("tp", sp), P(), P()),
            out_specs=cut,
            check_vma=False,
        )(queries, keys, *others)

    return layer
```

time: 705 us -> 345 us (0.49)
  waiting for transfers between devices: 583 us -> 226 us
  blocking collectives: 2.47 us -> 49.6 us
  matrix products: 52 us -> 18.8 us
  other arithmetic: 28.7 us -> 9.64 us
  local copies, waits for them, and re-layouts: 24.6 us -> 7.37 us
  Pallas kernels: 0 us -> 14.6 us
    all_gather x4 -> x5, waiting for transfers between devices: 557 us -> 169 us  [the longest x1 74.2 us: local(): down_full = lax.all_gather(down_own, 'w', axis=0)]
    all_to_all x0 -> x4, blocking collectives: none -> 49.6 us  [the longest x1 16.6 us: local(): down_own = lax.all_to_all(down_weight, 'a', 0, 1, tiled=True)]
    reduce_scatter x1, waiting for transfers between devices: 6.67 us -> 49.8 us  [local(): lax.psum_scatter(partial_ffn, ('a', 'tp'), scatter_dimension=0, tiled=True)]
    dot_general x6 -> x7, matrix products: 52 us -> 18.8 us  [the longest x1 7.95 us: local(): up_acts = jnp.dot(full_rows, up_full, preferred_element_type=jnp.float32)]
    reduce_sum x3 -> x0, other arithmetic: 17.5 us -> none  [the longest x2 16 us: advance(): totals = totals * factor + jnp.sum(weights, -1)]
    psum x1 -> x0, waiting for transfers between devices: 17 us -> none  [local(): lax.psum(partial_value.astype(jnp.bfloat16), 'tp').astype(jnp.float32)]
    pallas_call x0 -> x1, Pallas kernels: none -> 14.6 us  [attend(): pl.pallas_call(functools.partial(attend_kernel, chunk), grid=(heads, rows...]
    reshape x2 -> x0, local copies, waits for them, and re-layouts: 11.5 us -> none  [the longest x1 7.06 us: local(): value_piece.reshape(key_count // block_len, block_len, kv_heads, HEAD_SIZE)]
  transfers between devices with their start and end apart: 6 -> 7, of which waited for: 6 -> 6; matrix products, arithmetic and copies ran while one was open for 2% -> 5% of each run, Pallas kernels for 0% -> 4%
where the time goes in v1:
time: 345 us; the launch traced here: 344 us
  waiting for transfers between devices  226 us (66%)
  blocking collectives  49.6 us (14%)
  matrix products  18.8 us (5%)
  Pallas kernels  14.6 us (4%)
  between operations  13.8 us (4%)
  other arithmetic  9.64 us (3%)
  local copies, waits for them, and re-layouts  7.37 us (2%)
  starting transfers between devices  4.18 us (1%)
    all_gather x1, waiting for transfers between devices, local(): down_full = lax.all_gather(down_own, 'w', axis=0)  74.2 us
    reduce_scatter x1, waiting for transfers between devices, local(): lax.psum_scatter(partial_ffn, ('a', 'tp'), scatter_dimension=0, tiled=True)  49.8 us
    all_gather x1, waiting for transfers between devices, local(): up_full = lax.all_gather(up_own, 'w', axis=0, tiled=True)  48 us
    all_gather x1, waiting for transfers between devices, local(): full_rows = lax.all_gather(normed, ('a', 'tp'), axis=0, tiled=True)  36.8 us
    all_to_all x1, blocking collectives, local(): down_own = lax.all_to_all(down_weight, 'a', 0, 1, tiled=True)  16.6 us
    all_to_all x1, blocking collectives, local(): up_own = lax.all_to_all(up_weight, 'a', 1, 0, tiled=True)  15.4 us
    pallas_call x1, Pallas kernels, attend(): pl.pallas_call(functools.partial(attend_kernel, chunk), grid=(heads, rows...  14.6 us
    all_to_all x1, blocking collectives, local(): packed = lax.all_to_all(packed, 'a', 0, 0, tiled=True)  13.5 us
  transfers between devices with their start and end apart: 7, of which 6 were waited for; matrix products, arithmetic and copies ran while one was open for 5% of the time, Pallas kernels for 4%

profile of v1, /device:TPU:0, one launch (start us, length us, event | category | flops | bytes accessed | tf_op | source)
XLA Modules:
  0.0 344.2 jit_solution(14006931673082294758)
XLA Ops:
  6.5 0.0 all-gather.6.cloned.1.call-start
  6.6 1.2 copy.43
  7.7 0.1 fusion.7
  7.8 0.8 fusion.8
  8.6 0.2 multiply_cosine_fusion.1
  8.8 0.1 multiply_subtract_fusion.1
  8.9 0.0 copy-start
  9.0 0.0 copy-done.5
  9.0 0.1 copy.44
  9.2 0.0 copy-done.9
  9.2 0.1 fusion.11
  9.3 0.0 copy-done.6
  9.4 0.1 copy.45
  9.5 13.5 %all_to_all.64 = bf16[4,1,256,256]{2,3,1,0:T(8,128)(2,1)S(1)} all-to-all(bf16[4,1,256,256]{2,3,1,0:T(8,128)(2,1)S(1)} %bitcast.75), channel_id=1, replica_groups=mesh['w'=4,'a'=4,'tp'=2] {'a'}, dimensions={0} | all-to-all | bytes 1048576 | tf_op jit(solution)/shard_map/all_to_all | solution.py:158
  23.0 0.2 copy.47
  23.2 0.8 fusion.19
  24.0 0.0 all-gather.6.cloned.1.call-update
  24.1 0.0 all-gather.8.cloned.1.call-start
  24.1 0.7 all-gather.8.cloned.1.call-update
  24.8 0.0 all-gather.12.cloned.1.call-start
  24.9 0.0 copy-done
  24.9 0.7 copy.50
  25.6 15.4 %all_to_all.65 = bf16[128,4,1024]{0,2,1:T(8,128)(2,1)S(1)} all-to-all(bf16[128,4,1024]{0,2,1:T(8,128)(2,1)S(1)} %bitcast.69), channel_id=1, replica_groups=mesh['w'=4,'a'=4,'tp'=2] {'a'}, dimensions={1} | all-to-all | bytes 2097152 | tf_op jit(solution)/shard_map/all_to_all | solution.py:166
  40.9 1.3 copy.51
  42.3 0.0 all-gather.12.cloned.1.call-update
  42.3 9.6 %all-gather.6.cloned.1.call-done.kv_ref = bf16[1,4096,128]{2,1,0:T(8,128)(2,1)} async-done(((bf16[1,1024,128]{2,1,0:T(8,128)(2,1)}), bf16[1,4096,128]{2,1,0:T(8,128)(2,1)}) %all-gather.6.cloned.1.call-update) | async-done | bytes 1048592 | tf_op jit(solution)/shard_map/all_gather | solution.py:163
  51.9 14.6 %shard_map.127 = bf16[1,1024,128]{2,1,0:T(8,128)(2,1)} custom-call(bf16[1,1024,128]{2,1,0:T(8,128)(2,1)} %get-tuple-element.10.q_ref, bf16[1,4096,128]{2,1,0:T(8,128)(2,1)} %all-gather.6.cloned.1.call-done.kv_ref), custom_call_target="tpu_custom_call" | custom-call | flops 4294967296 | bytes 1572864 | tf_op jit(solution)/shard_map/pallas_call | solution.py:109
  66.6 3.8 %all-to-all-start.1 = ((bf16[8,1,128,128]{3,2,1,0:T(8,128)(2,1)}), bf16[8,1,128,128]{3,2,1,0:T(8,128)(2,1)S(1)}, u32[]{:S(2)}, u32[]{:S(2)}) async-start(bf16[8,1,128,128]{3,2,1,0:T(8,128)(2,1)} %bitcast.82), calls=%async_computation.1 | async-start | bytes 524288 | tf_op jit(solution)/shard_map/all_to_all | solution.py:175
  70.3 0.0 all-gather.10.cloned.1.call-start
  70.4 6.9 %all-to-all-done.1 = bf16[8,1,128,128]{3,2,1,0:T(8,128)(2,1)S(1)} async-done(((bf16[8,1,128,128]{3,2,1,0:T(8,128)(2,1)}), bf16[8,1,128,128]{3,2,1,0:T(8,128)(2,1)S(1)}, u32[]{:S(2)}, u32[]{:S(2)}) %all-to-all-start.1) | async-done | bytes 262176 | tf_op jit(solution)/shard_map/all_to_all | solution.py:175
  77.3 0.2 copy.49
  77.4 0.0 all-gather.8.cloned.1.call-done
  77.5 0.0 copy-start.3
  77.5 0.0 copy-start.4
  77.5 2.2 fusion.3
  79.7 0.0 copy-done.2
  79.7 0.0 copy-start.1
  79.7 2.3 fusion.20
  82.0 0.3 multiply_reduce_fusion.1
  82.3 1.0 add_convert_fusion.1
  83.3 0.0 all-gather.10.cloned.1.call-update
  83.3 0.0 all-gather.14.cloned.1.call-start
  83.4 16.6 %all_to_all.66 = bf16[4,1024,128]{2,1,0:T(8,128)(2,1)S(1)} all-to-all(bf16[4,1024,128]{2,1,0:T(8,128)(2,1)S(1)} %bitcast.77), channel_id=1, replica_groups=mesh['w'=4,'a'=4,'tp'=2] {'a'}, dimensions={0} | all-to-all | bytes 2097152 | tf_op jit(solution)/shard_map/all_to_all | solution.py:168
  99.9 0.5 copy.52
  100.5 1.3 copy.53
  101.8 0.0 all-gather.14.cloned.1.call-update
  101.8 0.2 reduce-scatter.2.cloned.1.call-start
  102.1 48.0 %all-gather.12.cloned.1.call-done = bf16[2048,1024]{1,0:T(8,128)(2,1)} async-done(((bf16[512,1024]{1,0:T(8,128)(2,1)}), bf16[2048,1024]{1,0:T(8,128)(2,1)}) %all-gather.12.cloned.1.call-update) | async-done | bytes 4194320 | tf_op jit(solution)/shard_map/all_gather | solution.py:167
  150.1 36.8 %all-gather.10.cloned.1.call-done = bf16[1024,2048]{1,0:T(8,128)(2,1)} async-done(((bf16[128,2048]{1,0:T(8,128)(2,1)}), bf16[1024,2048]{1,0:T(8,128)(2,1)}) %all-gather.10.cloned.1.call-update) | async-done | bytes 4194320 | tf_op jit(solution)/shard_map/all_gather | solution.py:190
  186.9 8.0 %multiply_convert_fusion = bf16[1024,1024]{1,0:T(8,128)(2,1)S(1)} fusion(bf16[1024,2048]{1,0:T(8,128)(2,1)} %all-gather.10.cloned.1.call-done, bf16[2048,1024]{1,0:T(8,128)(2,1)} %all-gather.12.cloned.1.call-done), kind=kOutput, calls=%fused_computation.1 | convolution fusion | flops 4298113024 | bytes 10485760 | tf_op jit(solution)/shard_map/dot_general | solution.py:191
  194.9 74.2 %all-gather.14.cloned.1.call-done = bf16[4,1024,512]{2,1,0:T(8,128)(2,1)} async-done(((bf16[1,1024,512]{2,1,0:T(8,128)(2,1)}), bf16[4,1024,512]{2,1,0:T(8,128)(2,1)}) %all-gather.14.cloned.1.call-update) | async-done | bytes 4194320 | tf_op jit(solution)/shard_map/all_gather | solution.py:169
  269.1 2.6 convolution_convert_fusion.2
  271.7 0.0 copy-done.10
  271.7 1.3 convolution_convert_fusion.3
  273.0 1.2 convolution_convert_fusion.4
  274.2 1.2 convolution_convert_fusion.5
  275.5 2.3 pad_maximum_fusion
  277.8 0.0 reduce-scatter.2.cloned.1.call-update
  277.8 49.8 %reduce-scatter.2.cloned.1.call-done = bf16[128,2048]{1,0:T(8,128)(2,1)} async-done(((bf16[1024,2048]{1,0:T(8,128)(2,1)}), bf16[128,2048]{1,0:T(8,128)(2,1)}) %reduce-scatter.2.cloned.1.call-update) | async-done | bytes 524304 | tf_op jit(solution)/shard_map/reduce_scatter | solution.py:200
  327.6 1.5 fusion.6
  329.1 1.5 multiply_reduce_fusion
  330.7 1.6 add_convert_fusion
  332.4 4.2 %all_to_all.67 = bf16[128,2,1024]{2,0,1:T(8,128)(2,1)S(1)} all-to-all(bf16[128,2,1024]{2,0,1:T(8,128)(2,1)S(1)} %bitcast.73), channel_id=1, replica_groups=mesh['w'=4,'a'=4,'tp'=2] {'tp'}, dimensions={1} | all-to-all | bytes 1048576 | tf_op jit(solution)/shard_map/all_to_all | solution.py:206
  336.5 0.8 copy.72
  (29 shorter events, 0.3 us)
Async XLA Ops:
  6.5 2.4 copy-start.5
  6.5 2.6 copy-start.9
  6.5 2.8 copy-start.6
  6.5 45.4 %all-gather.6.cloned.1.call-start = ((), (), s32[]{:S(2)}) async-start(), calls=%async_computation.6 | async-start | bytes 1310720 | tf_op jit(solution)/shard_map/all_gather | solution.py:163
  8.9 15.9 %copy-start = (bf16[128,4096]{1,0:T(8,128)(2,1)S(1)}, bf16[128,4096]{1,0:T(8,128)(2,1)}, u32[]{:S(2)}) copy-start(bf16[128,4096]{1,0:T(8,128)(2,1)} %param.22) | copy-start | bytes 3145732
  24.1 53.4 %all-gather.8.cloned.1.call-start = ((), (), s32[]{:S(2)}) async-start(), calls=%async_computation.7 | async-start | bytes 6291456 | tf_op jit(solution)/shard_map/all_gather | solution.py:165
  24.8 125.2 %all-gather.12.cloned.1.call-start = ((), (), s32[]{:S(2)}) async-start(), calls=%async_computation.9 | async-start | bytes 5242880 | tf_op jit(solution)/shard_map/all_gather | solution.py:167
  66.6 13.1 %copy-start.2 = (bf16[256,2048]{1,0:T(8,128)(2,1)S(1)}, bf16[256,2048]{1,0:T(8,128)(2,1)}, u32[]{:S(2)}) copy-start(bf16[256,2048]{1,0:T(8,128)(2,1)} %param.19) | copy-start | bytes 3145732
  66.6 10.7 %all-to-all-start.1 = ((bf16[8,1,128,128]{3,2,1,0:T(8,128)(2,1)}), bf16[8,1,128,128]{3,2,1,0:T(8,128)(2,1)S(1)}, u32[]{:S(2)}, u32[]{:S(2)}) async-start(bf16[8,1,128,128]{3,2,1,0:T(8,128)(2,1)} %bitcast.82), calls=%async_computation.1 | async-start | bytes 524288 | tf_op jit(solution)/shard_map/all_to_all | solution.py:175
  70.3 116.6 %all-gather.10.cloned.1.call-start = ((), (), s32[]{:S(2)}) async-start(), calls=%async_computation.8 | async-start | bytes 4718592 | tf_op jit(solution)/shard_map/all_gather | solution.py:190
  77.5 4.8 %copy-start.3 = (f32[2048]{0:T(1024)S(1)}, f32[2048]{0:T(1024)}, u32[]{:S(2)}) copy-start(f32[2048]{0:T(1024)} %param.21) | copy-start | bytes 24580
  77.5 4.8 %copy-start.4 = (f32[2048]{0:T(1024)S(1)}, f32[2048]{0:T(1024)}, u32[]{:S(2)}) copy-start(f32[2048]{0:T(1024)} %param.20) | copy-start | bytes 24580
  79.7 3.7 %copy-start.1 = (bf16[4096,128]{1,0:T(8,128)(2,1)S(1)}, bf16[4096,128]{1,0:T(8,128)(2,1)}, u32[]{:S(2)}) copy-start(bf16[4096,128]{1,0:T(8,128)(2,1)} %param.23) | copy-start | bytes 3145732
  83.3 185.8 %all-gather.14.cloned.1.call-start = ((), (), s32[]{:S(2)}) async-start(), calls=%async_computation.10 | async-start | bytes 5242880 | tf_op jit(solution)/shard_map/all_gather | solution.py:169
  101.8 225.8 %reduce-scatter.2.cloned.1.call-start = ((), (), s32[]{:S(2)}) async-start(), calls=%async_computation.11 | async-start | bytes 4718592 | tf_op jit(solution)/shard_map/reduce_scatter | solution.py:200
  269.1 2.6 copy-start.10
  277.8 52.9 %copy-start.7 = (f32[2048]{0:T(1024)S(1)}, f32[2048]{0:T(1024)}, u32[]{:S(2)}) copy-start(f32[2048]{0:T(1024)} %param.25) | copy-start | bytes 24580
  277.8 52.9 %copy-start.8 = (f32[2048]{0:T(1024)S(1)}, f32[2048]{0:T(1024)}, u32[]{:S(2)}) copy-start(f32[2048]{0:T(1024)} %param.24) | copy-start | bytes 24580
Sparse Core Ops, SparseCore 0:
  24.2 27.6 all-gather.5
  53.5 13.0 all-gather.7
  68.1 81.9 all-gather.11
  151.8 35.0 all-gather.9
  188.3 80.7 all-gather.13
  277.9 49.6 reduce-scatter.1

commit v2 on v1

--- a/solution.py
+++ b/solution.py
@@ -142,7 +142,7 @@
 ):
     tok_rows = queries.shape[0]
     n_a, n_tp = lax.axis_size("a"), lax.axis_size("tp")
-    grid_places = lax.axis_index(("w", "a")) * tok_rows + jnp.arange(tok_rows, dtype=jnp.int32)
+    grid_places = lax.axis_index(("a", "w")) * tok_rows + jnp.arange(tok_rows, dtype=jnp.int32)
     kv_heads = keys.shape[1] // HEAD_SIZE
     q_count = queries.shape[1] // HEAD_SIZE
     own_heads = kv_heads // n_a
@@ -187,7 +187,9 @@
     normed = layer_norm(
         ALPHA * own_residual.astype(jnp.float32) + mixed, ln1_gain, ln1_bias
     ).astype(jnp.bfloat16)
-    full_rows = lax.all_gather(normed, ("a", "tp"), axis=0, tiled=True)
+    n_w = lax.axis_size("w")
+    turned = normed.reshape(rows, n_a, n_w, -1).swapaxes(1, 2).reshape(rows, D)
+    full_rows = lax.all_gather(turned, ("a", "tp"), axis=0, tiled=True)
     up_acts = jnp.dot(full_rows, up_full, preferred_element_type=jnp.float32)
     hidden = jnp.square(jnp.maximum(up_acts, 0.0)).astype(jnp.bfloat16)
     partial_ffn = jnp.concatenate(
@@ -199,7 +201,10 @@
     )
     ffn_out = lax.psum_scatter(
         partial_ffn, ("a", "tp"), scatter_dimension=0, tiled=True
-    ).astype(jnp.float32)
+    )
+    ffn_out = (
+        ffn_out.reshape(rows, n_w, n_a, -1).swapaxes(1, 2).reshape(rows, D).astype(jnp.float32)
+    )
     encoded = layer_norm(
         ALPHA * normed.astype(jnp.float32) + ffn_out, ln2_gain, ln2_bias
     ).astype(jnp.bfloat16)
@@ -211,8 +216,8 @@
 
     def layer(queries, keys, *others):
         n_a = math.gcd(n_sp, keys.shape[1] // (HEAD_SIZE * n_tp))
-        groups = Mesh(mesh.devices.reshape(n_sp // n_a, n_a, n_tp), ("w", "a", "tp"))
-        sp = ("w", "a")
+        groups = Mesh(mesh.devices.reshape(n_a, n_sp // n_a, n_tp), ("a", "w", "tp"))
+        sp = ("a", "w")
         cut = P(sp, "tp")
         return jax.shard_map(
             local,

time: 345 us -> 311 us (0.901)
  waiting for transfers between devices: 226 us -> 154 us
  blocking collectives: 49.6 us -> 81.8 us
  local copies, waits for them, and re-layouts: 7.37 us -> 17.7 us
  other arithmetic: 9.64 us -> 5.64 us
    unnamed x6 -> x7, waiting for transfers between devices: 0.78 us -> 50.9 us
    reduce_scatter x1 -> x0, waiting for transfers between devices: 49.8 us -> none  [local(): lax.psum_scatter(partial_ffn, ('a', 'tp'), scatter_dimension=0, tiled=True)]
    all_gather x1, waiting for transfers between devices: 48 us -> 0.05 us  [local(): up_full = lax.all_gather(up_own, 'w', axis=0, tiled=True)]
    all_gather x1, waiting for transfers between devices: 74.2 us -> 44.4 us  [local(): down_full = lax.all_gather(down_own, 'w', axis=0)]
    all_to_all x1, blocking collectives: 16.6 us -> 29.2 us  [local(): down_own = lax.all_to_all(down_weight, 'a', 0, 1, tiled=True)]
    all_to_all x1, blocking collectives: 15.4 us -> 27.8 us  [local(): up_own = lax.all_to_all(up_weight, 'a', 1, 0, tiled=True)]
    all_gather x1, waiting for transfers between devices: 36.8 us -> 49.3 us  [local(): full_rows = lax.all_gather(turned, ('a', 'tp'), axis=0, tiled=True)]
    all_gather x1, waiting for transfers between devices: 9.62 us -> 0.02 us  [local(): kv = lax.all_gather(packed[..., 2 * HEAD_SIZE:], 'w', axis=1, tiled=True)]
  transfers between devices with their start and end apart: 7 -> 7, of which waited for: 6 -> 4; matrix products, arithmetic and copies ran while one was open for 5% -> 6% of each run, Pallas kernels for 4% -> 5%
where the time goes in v2:
time: 311 us
  waiting for transfers between devices  154 us (50%)
  blocking collectives  81.8 us (26%)
  matrix products  18.9 us (6%)
  local copies, waits for them, and re-layouts  17.7 us (6%)
  Pallas kernels  14.7 us (5%)
  between operations  13.9 us (4%)
  other arithmetic  5.64 us (2%)
  starting transfers between devices  3.93 us (1%)
    unnamed x7, waiting for transfers between devices  50.9 us
    all_gather x1, waiting for transfers between devices, local(): full_rows = lax.all_gather(turned, ('a', 'tp'), axis=0, tiled=True)  49.3 us
    all_gather x1, waiting for transfers between devices, local(): down_full = lax.all_gather(down_own, 'w', axis=0)  44.4 us
    all_to_all x1, blocking collectives, local(): down_own = lax.all_to_all(down_weight, 'a', 0, 1, tiled=True)  29.2 us
    all_to_all x1, blocking collectives, local(): up_own = lax.all_to_all(up_weight, 'a', 1, 0, tiled=True)  27.8 us
    all_to_all x1, blocking collectives, local(): packed = lax.all_to_all(packed, 'a', 0, 0, tiled=True)  20.6 us
    pallas_call x1, Pallas kernels, attend(): pl.pallas_call(functools.partial(attend_kernel, chunk), grid=(heads, rows...  14.7 us
    unnamed x28, local copies, waits for them, and re-layouts  10.7 us
  transfers between devices with their start and end apart: 7, of which 4 were waited for; matrix products, arithmetic and copies ran while one was open for 6% of the time, Pallas kernels for 5%

profile of v2, /device:TPU:0, one launch (start us, length us, event | category | flops | bytes accessed | tf_op | source)
XLA Modules:
  0.0 310.8 jit_solution(6972868588431181497)
XLA Ops:
  6.6 1.2 copy.36
  7.7 0.1 fusion.6
  7.8 0.8 fusion.7
  8.6 0.2 multiply_cosine_fusion.1
  8.8 0.1 multiply_subtract_fusion.1
  8.9 0.0 copy-start
  9.0 0.1 copy.37
  9.2 0.1 fusion.11
  9.4 0.1 copy.38
  9.5 20.6 %all_to_all.64 = bf16[4,1,256,256]{2,3,1,0:T(8,128)(2,1)S(1)} all-to-all(bf16[4,1,256,256]{2,3,1,0:T(8,128)(2,1)S(1)} %bitcast.85), channel_id=1, replica_groups=mesh['a'=4,'w'=4,'tp'=2] {'a'}, dimensions={0} | all-to-all | bytes 1048576 | tf_op jit(solution)/shard_map/all_to_all | solution.py:158
  30.1 0.2 copy.40
  30.3 0.8 fusion.19
  31.2 0.0 all-gather.6.cloned.1.call-update
  31.2 0.0 all-gather.8.cloned.1.call-start
  31.2 0.7 all-gather.8.cloned.1.call-update
  31.9 0.0 all-gather.12.cloned.1.call-start
  32.0 0.7 copy.44
  32.7 27.8 %all_to_all.65 = bf16[128,4,1024]{0,2,1:T(8,128)(2,1)S(1)} all-to-all(bf16[128,4,1024]{0,2,1:T(8,128)(2,1)S(1)} %bitcast.77), channel_id=1, replica_groups=mesh['a'=4,'w'=4,'tp'=2] {'a'}, dimensions={1} | all-to-all | bytes 2097152 | tf_op jit(solution)/shard_map/all_to_all | solution.py:166
  60.5 1.3 copy.45
  61.8 0.0 all-gather.12.cloned.1.call-update
  61.9 0.0 all-gather.6.cloned.1.call-done.kv_ref
  61.9 14.7 %shard_map.127 = bf16[1,1024,128]{2,1,0:T(8,128)(2,1)} custom-call(bf16[1,1024,128]{2,1,0:T(8,128)(2,1)} %get-tuple-element.10.q_ref, bf16[1,4096,128]{2,1,0:T(8,128)(2,1)} %all-gather.6.cloned.1.call-done.kv_ref), custom_call_target="tpu_custom_call" | custom-call | flops 4294967296 | bytes 1572864 | tf_op jit(solution)/shard_map/pallas_call | solution.py:109
  76.5 3.5 %all-to-all-start.1 = ((bf16[8,1,128,128]{3,2,1,0:T(8,128)(2,1)}), bf16[8,1,128,128]{3,2,1,0:T(8,128)(2,1)S(1)}, u32[]{:S(2)}, u32[]{:S(2)}) async-start(bf16[8,1,128,128]{3,2,1,0:T(8,128)(2,1)} %bitcast.92), calls=%async_computation.1 | async-start | bytes 524288 | tf_op jit(solution)/shard_map/all_to_all | solution.py:175
  80.1 0.0 all-gather.10.cloned.1.call-start
  80.1 9.6 %all-to-all-done.1 = bf16[8,1,128,128]{3,2,1,0:T(8,128)(2,1)S(1)} async-done(((bf16[8,1,128,128]{3,2,1,0:T(8,128)(2,1)}), bf16[8,1,128,128]{3,2,1,0:T(8,128)(2,1)S(1)}, u32[]{:S(2)}, u32[]{:S(2)}) %all-to-all-start.1) | async-done | bytes 262176 | tf_op jit(solution)/shard_map/all_to_all | solution.py:175
  89.7 0.2 copy.42
  89.9 0.0 all-gather.8.cloned.1.call-done
  89.9 0.0 copy-start.2
  89.9 0.0 copy-start.3
  90.0 2.1 fusion.3
  92.0 2.2 fusion.20
  94.2 0.3 multiply_reduce_fusion.1
  94.5 0.2 add_convert_fusion.1
  94.8 0.4 reshape.234
  95.1 1.2 copy.43
  96.4 0.0 all-gather.10.cloned.1.call-update
  96.4 0.0 all-gather.14.cloned.1.call-start
  96.4 29.2 %all_to_all.66 = bf16[4,1024,128]{2,1,0:T(8,128)(2,1)S(1)} all-to-all(bf16[4,1024,128]{2,1,0:T(8,128)(2,1)} %bitcast.87), channel_id=1, replica_groups=mesh['a'=4,'w'=4,'tp'=2] {'a'}, dimensions={0} | all-to-all | bytes 2097152 | tf_op jit(solution)/shard_map/all_to_all | solution.py:168
  125.6 0.5 copy.46
  126.2 1.3 copy.47
  127.5 0.0 all-gather.14.cloned.1.call-update
  127.5 0.2 reduce-scatter.4.cloned.1.call-start
  127.8 0.0 all-gather.12.cloned.1.call-done
  127.8 49.3 %all-gather.10.cloned.1.call-done = bf16[1024,2048]{0,1:T(8,128)(2,1)} async-done(((bf16[128,2048]{0,1:T(8,128)(2,1)}), bf16[1024,2048]{0,1:T(8,128)(2,1)}) %all-gather.10.cloned.1.call-update) | async-done | bytes 4194320 | tf_op jit(solution)/shard_map/all_gather | solution.py:192
  177.1 8.0 %multiply_convert_fusion = bf16[1024,1024]{1,0:T(8,128)(2,1)S(1)} fusion(bf16[1024,2048]{0,1:T(8,128)(2,1)} %all-gather.10.cloned.1.call-done, bf16[2048,1024]{1,0:T(8,128)(2,1)} %all-gather.12.cloned.1.call-done), kind=kOutput, calls=%fused_computation.1 | convolution fusion | flops 4298113024 | bytes 10485760 | tf_op jit(solution)/shard_map/dot_general | solution.py:193
  185.2 44.4 %all-gather.14.cloned.1.call-done = bf16[4,1024,512]{2,1,0:T(8,128)(2,1)} async-done(((bf16[1,1024,512]{2,1,0:T(8,128)(2,1)}), bf16[4,1024,512]{2,1,0:T(8,128)(2,1)}) %all-gather.14.cloned.1.call-update) | async-done | bytes 4194320 | tf_op jit(solution)/shard_map/all_gather | solution.py:169
  229.6 2.7 convolution_convert_fusion.2
  232.3 1.3 convolution_convert_fusion.3
  233.6 1.3 convolution_convert_fusion.4
  234.9 1.3 convolution_convert_fusion.5
  236.2 2.3 pad_maximum_fusion
  238.5 6.5 %copy.50 = bf16[1024,2048]{1,0:T(8,128)(2,1)} copy(bf16[1024,2048]{0,1:T(8,128)(2,1)} %pad_maximum_fusion) | data formatting | bytes 8388608
  245.0 0.0 reduce-scatter.4.cloned.1.call-update
  245.1 50.1 %reduce-scatter.4.cloned.1.call-done = bf16[128,2048]{1,0:T(8,128)(2,1)} async-done(((bf16[1024,2048]{1,0:T(8,128)(2,1)}), bf16[128,2048]{1,0:T(8,128)(2,1)}) %reduce-scatter.4.cloned.1.call-update) | async-done | bytes 524304
  295.2 1.3 copy.51
  296.5 0.0 copy-start.6
  296.5 0.0 copy-start.7
  296.5 0.5 copy.48
  297.1 0.4 reshape.238
  297.5 0.4 fusion.9
  297.9 0.5 multiply_reduce_fusion
  298.4 0.6 add_convert_fusion
  299.0 4.2 %all_to_all.67 = bf16[128,2,1024]{2,0,1:T(8,128)(2,1)S(1)} all-to-all(bf16[128,2,1024]{2,0,1:T(8,128)(2,1)S(1)} %bitcast.82), channel_id=1, replica_groups=mesh['a'=4,'w'=4,'tp'=2] {'tp'}, dimensions={1} | all-to-all | bytes 1048576 | tf_op jit(solution)/shard_map/all_to_all | solution.py:211
  303.2 0.8 copy.61
  (33 shorter events, 0.3 us)
Async XLA Ops:
  6.5 2.4 copy-start.4
  6.5 2.6 copy-start.8
  6.5 2.8 copy-start.5
  6.5 55.3 %all-gather.6.cloned.1.call-start = ((), (), s32[]{:S(2)}) async-start(), calls=%async_computation.6 | async-start | bytes 1310720 | tf_op jit(solution)/shard_map/all_gather | solution.py:163
  8.9 23.0 %copy-start = (bf16[128,4096]{1,0:T(8,128)(2,1)S(1)}, bf16[128,4096]{1,0:T(8,128)(2,1)}, u32[]{:S(2)}) copy-start(bf16[128,4096]{1,0:T(8,128)(2,1)} %param.22) | copy-start | bytes 3145732
  31.2 58.7 %all-gather.8.cloned.1.call-start = ((), (), s32[]{:S(2)}) async-start(), calls=%async_computation.7 | async-start | bytes 6291456 | tf_op jit(solution)/shard_map/all_gather | solution.py:165
  31.9 95.9 %all-gather.12.cloned.1.call-start = ((), (), s32[]{:S(2)}) async-start(), calls=%async_computation.9 | async-start | bytes 5242880 | tf_op jit(solution)/shard_map/all_gather | solution.py:167
  76.5 15.5 %copy-start.1 = (bf16[256,2048]{1,0:T(8,128)(2,1)S(1)}, bf16[256,2048]{1,0:T(8,128)(2,1)}, u32[]{:S(2)}) copy-start(bf16[256,2048]{1,0:T(8,128)(2,1)} %param.19) | copy-start | bytes 3145732
  76.5 13.2 %all-to-all-start.1 = ((bf16[8,1,128,128]{3,2,1,0:T(8,128)(2,1)}), bf16[8,1,128,128]{3,2,1,0:T(8,128)(2,1)S(1)}, u32[]{:S(2)}, u32[]{:S(2)}) async-start(bf16[8,1,128,128]{3,2,1,0:T(8,128)(2,1)} %bitcast.92), calls=%async_computation.1 | async-start | bytes 524288 | tf_op jit(solution)/shard_map/all_to_all | solution.py:175
  80.1 97.0 %all-gather.10.cloned.1.call-start = ((), (), s32[]{:S(2)}) async-start(), calls=%async_computation.8 | async-start | bytes 4718592 | tf_op jit(solution)/shard_map/all_gather | solution.py:192
  89.9 4.6 %copy-start.2 = (f32[2048]{0:T(1024)S(1)}, f32[2048]{0:T(1024)}, u32[]{:S(2)}) copy-start(f32[2048]{0:T(1024)} %param.21) | copy-start | bytes 24580
  89.9 4.6 %copy-start.3 = (f32[2048]{0:T(1024)S(1)}, f32[2048]{0:T(1024)}, u32[]{:S(2)}) copy-start(f32[2048]{0:T(1024)} %param.20) | copy-start | bytes 24580
  96.4 133.2 %all-gather.14.cloned.1.call-start = ((), (), s32[]{:S(2)}) async-start(), calls=%async_computation.10 | async-start | bytes 5242880 | tf_op jit(solution)/shard_map/all_gather | solution.py:169
  127.5 167.6 %reduce-scatter.4.cloned.1.call-start = ((), (), s32[]{:S(2)}) async-start(), calls=%async_computation.11 | async-start | bytes 4718592
  229.6 2.7 copy-start.9
  296.5 1.9 copy-start.6
  296.5 1.9 copy-start.7
Sparse Core Ops, SparseCore 0:
  31.3 25.5 all-gather.5
  58.5 13.6 all-gather.7
  74.0 53.7 all-gather.11
  129.2 47.8 all-gather.9
  178.8 50.7 all-gather.13
  245.2 49.9 reduce-scatter.3
